TPU v7x, 32 devices: a whole 2x2x4 slice. The times are simulated.
32 devices in a mesh: grp: 2 (over y), sp: 4 (over z), tp: 4 (over x, core).
Axes of the slice: x: 2, y: 2, z: 4, core: 2. Of those that a mesh axis runs over, the one named last changes fastest.
Arguments:
- stream: bfloat16 [2048, 2048], P(('grp', 'sp')), parts along dimension 0, may hold values from -6 to 6
- doc_ids: int32 [2048], P(('grp', 'sp')), parts along dimension 0, may hold values from 0 to 1, never falling along the last dimension, each value on 1 to 768 neighbouring positions
- norm_gain: float32 [2, 2048], replicated, may hold values from 0.1 to 1.9
- query_weight: bfloat16 [2, 2048, 1024], P(None, 'sp', 'tp'), may hold values from -0.125 to 0.125
- key_weight: bfloat16 [2, 2048, 1024], P(None, 'sp', 'tp'), may hold values from -0.125 to 0.125
- value_weight: bfloat16 [2, 2048, 1024], P(None, 'sp', 'tp'), may hold values from -0.125 to 0.125
- out_weight: bfloat16 [2, 1024, 2048], P(None, 'sp', 'tp'), may hold values from -0.75 to 0.75
- query_gain: float32 [2, 64], replicated, may hold values from 0.1 to 1.9
- key_gain: float32 [2, 64], replicated, may hold values from 0.1 to 1.9
- rel_bias: float32 [16, 513], P('tp'), may hold values from -4 to 250
Outputs:
- encoded: bfloat16 [2048, 2048], P(('grp', 'sp')), parts along dimension 0
There are 2 independent parts, one for each index of `grp`. A program takes and returns all parts, laid end to end along the dimension named above; an argument that names none is the same for every part. Nothing has to cross between parts.
Inputs may be any that keep to these rules, and one draw needn't show every extreme that they name: doc_ids never fall along the sequence; each document has at most 768 positions.
All inputs are finite; a program needn't handle non-finite values.
Results may differ from a plain program's by a relative error of at most 0.011.
Values may be sent and summed in bfloat16 or wider, within the bound.
A program may use at most 64 MiB of HBM per device.

v0:
```python
import jax
import jax.numpy as jnp
from jax import lax
from jax.sharding import PartitionSpec as P

SEG = 64
LEFT = 8
MAXREL = 256
LAYERS = 2


epsilon = 1e-06


def shifted(value, axis, steps):
    count = lax.axis_size(axis)
    initial, last = (max(0, -steps), min(count, count - steps))
    return lax.ppermute(value, axis, [(source, source + steps) for source in range(initial, last)])


def row_norm(values, gain):
    return values * lax.rsqrt(jnp.mean(values * values, axis=-1, keepdims=True) + epsilon) * gain


def bias_table(rel_bias):
    heads_here = rel_bias.shape[0]
    reach = LEFT * SEG
    width = (LEFT + 1) * SEG
    highest = reach + SEG - 1
    reversed_bias = rel_bias[:, ::-1]
    upper_fill = jnp.broadcast_to(rel_bias[:, -1:], (heads_here, highest - MAXREL))
    flat_row = jnp.concatenate([upper_fill, reversed_bias[:, : MAXREL + SEG]], axis=1)
    lines = [
        flat_row[:, SEG - 1 - position : SEG - 1 - position + width] for position in range(SEG)
    ]
    return jnp.stack(lines, axis=1)


def attend(query, ext_keys, ext_values, ext_docs, own_docs, offset, table):
    rows, heads_here, head_size = query.shape
    count = rows // SEG
    width = (LEFT + 1) * SEG
    blocks = query.reshape(count, SEG, heads_here, head_size)
    key_blocks = ext_keys.reshape(count + LEFT, SEG, heads_here, head_size)
    value_blocks = ext_values.reshape(count + LEFT, SEG, heads_here, head_size)
    doc_blocks = ext_docs.reshape(count + LEFT, SEG)
    score_parts = [
        jnp.einsum(
            "nqhd,nkhd->nhqk",
            blocks,
            key_blocks[earlier : earlier + count],
            preferred_element_type=jnp.float32,
        )
        for earlier in range(LEFT + 1)
    ]
    scores = jnp.concatenate(score_parts, axis=-1)
    scores = scores * head_size ** (-0.5) + table[None]
    doc_band = jnp.concatenate(
        [doc_blocks[earlier : earlier + count] for earlier in range(LEFT + 1)], axis=1
    )
    key_pos = (
        offset
        + SEG * jnp.arange(count, dtype=jnp.int32)[:, None]
        - LEFT * SEG
        + jnp.arange(width, dtype=jnp.int32)[None, :]
    )
    allowed = (key_pos >= 0)[:, None, None, :] & (
        doc_band[:, None, None, :] == own_docs.reshape(count, SEG)[:, None, :, None]
    )
    scores = jnp.where(allowed, scores, -1e30)
    peak = jnp.max(scores, axis=-1, keepdims=True)
    expo = jnp.exp(scores - peak)
    weights = (expo / jnp.sum(expo, axis=-1, keepdims=True)).astype(jnp.bfloat16)
    mixed = jnp.zeros((count, SEG, heads_here, head_size), jnp.float32)
    for earlier in range(LEFT + 1):
        part_weights = weights[..., earlier * SEG : (earlier + 1) * SEG]
        mixed = mixed + jnp.einsum(
            "nhqk,nkhd->nqhd",
            part_weights,
            value_blocks[earlier : earlier + count],
            preferred_element_type=jnp.float32,
        )
    return mixed.astype(jnp.bfloat16).reshape(rows, heads_here * head_size)


def on_device(
    stream,
    doc_ids,
    norm_gain,
    query_weight,
    key_weight,
    value_weight,
    out_weight,
    query_gain,
    key_gain,
    rel_bias,
):
    rows = stream.shape[0]
    heads_here = rel_bias.shape[0]
    head_size = query_gain.shape[1]
    local_width = heads_here * head_size
    reach = LEFT * SEG
    depth = -(-reach // rows)
    offset = lax.axis_index("sp") * rows
    col_width = out_weight.shape[2]
    col_start = lax.axis_index("tp") * col_width
    table = bias_table(rel_bias)
    x = stream
    for layer in range(LAYERS):
        widened = x.astype(jnp.float32)
        normed = row_norm(widened, norm_gain[layer]).astype(jnp.bfloat16)
        own_cols = normed
        q_raw = jnp.dot(
            own_cols,
            lax.all_gather(query_weight[layer], "sp", axis=0, tiled=True),
            preferred_element_type=jnp.float32,
        )
        k_raw = jnp.dot(
            normed,
            lax.all_gather(key_weight[layer], "sp", axis=0, tiled=True),
            preferred_element_type=jnp.float32,
        )
        v_raw = jnp.dot(
            normed,
            lax.all_gather(value_weight[layer], "sp", axis=0, tiled=True),
            preferred_element_type=jnp.float32,
        )
        query = row_norm(q_raw.reshape(rows, heads_here, head_size), query_gain[layer]).astype(
            jnp.bfloat16
        )
        keys = row_norm(
            k_raw.reshape(normed.shape[0], heads_here, head_size), key_gain[layer]
        ).astype(jnp.bfloat16)
        values = v_raw.astype(jnp.bfloat16)
        flat_keys = keys.reshape(rows, local_width)
        tail = (flat_keys, values, doc_ids)
        received = [
            shifted((tail[0], tail[1], tail[2]), "sp", distance_back)
            for distance_back in range(depth, 0, -1)
        ]
        ext_keys = jnp.concatenate([item[0] for item in received] + [flat_keys], axis=0)
        ext_values = jnp.concatenate([item[1] for item in received] + [values], axis=0)
        ext_docs = jnp.concatenate([item[2] for item in received] + [doc_ids], axis=0)
        ext_keys = ext_keys.reshape(reach + rows, heads_here, head_size)
        ext_values = ext_values.reshape(reach + rows, heads_here, head_size)
        attended = attend(query, ext_keys, ext_values, ext_docs, doc_ids, offset, table)
        all_heads = lax.all_gather(attended, "tp", axis=1, tiled=True)
        projected = jnp.dot(
            all_heads,
            lax.all_gather(out_weight[layer], "sp", axis=0, tiled=True),
            preferred_element_type=jnp.float32,
        )
        own_cols = lax.dynamic_slice_in_dim(widened, col_start, col_width, 1)
        new_cols = (own_cols + projected).astype(jnp.bfloat16)
        x = lax.all_gather(new_cols, "tp", axis=1, tiled=True)
    return x


def solution(mesh):
    placed = (
        P(("grp", "sp"), None),
        P(("grp", "sp")),
        P(),
        P(None, "sp", "tp"),
        P(None, "sp", "tp"),
        P(None, "sp", "tp"),
        P(None, "sp", "tp"),
        P(),
        P(),
        P("tp", None),
    )
    return jax.shard_map(
        on_device, mesh=mesh, in_specs=placed, out_specs=P(("grp", "sp"), None), check_vma=False
    )
```

profile of v0, /device:TPU:0, one launch (start us, length us, event | category | flops | bytes accessed | tf_op | source)
XLA Modules:
  0.0 338.0 jit_solution(15381538330978030332)
XLA Ops:
  6.5 2.0 fusion.257
  8.6 2.0 fusion.256
  11.6 6.0 %collective-permute-start.1 = (s32[256]{0:T(256)S(1)}, s32[256]{0:T(256)S(1)}, u32[]{:S(2)}, u32[]{:S(2)}) collective-permute-start(s32[256]{0:T(256)S(1)} %copy-done.17), channel_id=1, source_target_pairs={{0,8},{4,12},{1,9},{5,13},{2,10},{6,14},{3,11},{7,15},{16,24},{20,... | collective-permute-start | bytes 3080 | tf_op jit(solution)/shard_map/ppermute | solution.py:18
  17.5 3.5 %collective-permute-start.2 = (s32[256]{0:T(256)S(1)}, s32[256]{0:T(256)S(1)}, u32[]{:S(2)}, u32[]{:S(2)}) collective-permute-start(s32[256]{0:T(256)S(1)} %copy-done.17), channel_id=1, source_target_pairs={{0,4},{4,8},{8,12},{1,5},{5,9},{9,13},{2,6},{6,10},{10,14},{3,7},{... | collective-permute-start | bytes 3080 | tf_op jit(solution)/shard_map/ppermute | solution.py:18
  28.4 1.6 convert_element_type.52
  30.6 9.0 %all-gather.27.cloned.1.call-done = bf16[1,2048,256]{2,1,0:T(8,128)(2,1)} async-done(((bf16[1,512,256]{2,1,0:T(8,128)(2,1)}), bf16[1,2048,256]{2,1,0:T(8,128)(2,1)}) %all-gather.27.cloned.1.call-update) | async-done | bytes 1048592 | tf_op jit(solution)/shard_map/all_gather | solution.py:120
  39.7 1.9 bitcast_reduce_fusion.2
  41.7 3.7 %collective-permute-start.3 = (bf16[256,256]{0,1:T(8,128)(2,1)S(1)}, bf16[256,256]{0,1:T(8,128)(2,1)S(1)}, u32[]{:S(2)}, u32[]{:S(2)}) collective-permute-start(bf16[256,256]{0,1:T(8,128)(2,1)S(1)} %fusion.61), channel_id=1, source_target_pairs={{0,8},{4,12},{1,9},{5,13},{2,10},{6,14},{3,11},{7,15},{16,24},{20,... | collective-permute-start | bytes 393224 | tf_op jit(solution)/shard_map/ppermute | solution.py:18
  45.4 2.5 collective-permute-start.4
  48.0 20.7 %all-gather.23.cloned.1.call-done = bf16[1,2048,256]{2,1,0:T(8,128)(2,1)} async-done(((bf16[1,512,256]{2,1,0:T(8,128)(2,1)}), bf16[1,2048,256]{2,1,0:T(8,128)(2,1)}) %all-gather.23.cloned.1.call-update) | async-done | bytes 1048592 | tf_op jit(solution)/shard_map/all_gather | solution.py:125
  68.8 1.7 convolution_convert_fusion.1
  70.5 5.6 %collective-permute-start.5 = (bf16[256,256]{1,0:T(8,128)(2,1)S(1)}, bf16[256,256]{1,0:T(8,128)(2,1)S(1)}, u32[]{:S(2)}, u32[]{:S(2)}) collective-permute-start(bf16[256,256]{1,0:T(8,128)(2,1)S(1)} %convolution_convert_fusion.1), channel_id=1, source_target_pairs={{0,4},{4,8},{8,12},{1,5},{5,9},{9,13},{2,6},{6,10},{10,14},{3,7},{... | collective-permute-start | bytes 393224 | tf_op jit(solution)/shard_map/ppermute | solution.py:18
  76.1 4.3 %collective-permute-start = (bf16[256,256]{1,0:T(8,128)(2,1)S(1)}, bf16[256,256]{1,0:T(8,128)(2,1)S(1)}, u32[]{:S(2)}, u32[]{:S(2)}) collective-permute-start(bf16[256,256]{1,0:T(8,128)(2,1)S(1)} %convolution_convert_fusion.1), channel_id=1, source_target_pairs={{0,8},{4,12},{1,9},{5,13},{2,10},{6,14},{3,11},{7,15},{16,24},{20,... | collective-permute-start | bytes 393224 | tf_op jit(solution)/shard_map/ppermute | solution.py:18
  81.3 19.7 %all-gather.25.cloned.1.call-done = bf16[1,2048,256]{2,1,0:T(8,128)(2,1)} async-done(((bf16[1,512,256]{2,1,0:T(8,128)(2,1)}), bf16[1,2048,256]{2,1,0:T(8,128)(2,1)}) %all-gather.25.cloned.1.call-update) | async-done | bytes 1048592 | tf_op jit(solution)/shard_map/all_gather | solution.py:115
  101.0 1.9 bitcast_reduce_fusion.3
  103.7 1.0 fusion.98
  108.8 1.0 fusion.108
  110.0 1.1 fusion.106
  111.2 1.0 fusion.104
  118.7 3.6 %concatenate.92 = f32[4,4,64,576]{3,2,1,0:T(8,128)S(1)} concatenate(f32[4,4,64,64]{3,2,1,0:T(8,128)} %fusion.114, f32[4,4,64,64]{3,2,1,0:T(8,128)} %fusion.112, f32[4,4,64,64]{3,2,1,0:T(8,128)} %fusion.110, f32[4,4,64,64]{3,2,1,0:T(8,128)} %fusion.108, f32[4,4,64,64]{3,2,1,0:T(8,128)} %fusion.106, f32[4,4,64,64]{3,2,1,0:T(8,128)} %fusion.104, f32[4,4,64,64]{3,2,1,0:T(8,128)} %fusion.102, ...), dimensions={3} | concatenate | bytes 4718592 | tf_op jit(solution)/shard_map/concatenate | solution.py:56
  125.0 1.8 slice.569
  126.8 1.3 fusion.15
  128.0 1.3 fusion.49
  129.3 1.8 slice.670
  131.1 1.1 slice.678
  132.2 1.1 slice.681
  133.3 1.8 slice.672
  135.1 1.3 convolution_add_fusion.12
  136.4 1.3 fusion.14
  139.4 8.7 %all_gather.39 = bf16[256,1024]{1,0:T(8,128)(2,1)S(1)} all-gather(bf16[256,256]{1,0:T(8,128)(2,1)S(1)} %reshape.224), channel_id=1, replica_groups=mesh['grp'=2,'sp'=4,'tp'=4] {'tp'}, dimensions={1}, use_global_device_ids=true | all-gather | bytes 655360 | tf_op jit(solution)/shard_map/all_gather | solution.py:147
  148.1 2.5 fusion.16
  153.6 15.3 %all-gather.19.cloned.1.call-done = bf16[256,2048]{1,0:T(8,128)(2,1)} async-done(((bf16[256,512]{1,0:T(8,128)(2,1)}), bf16[256,2048]{1,0:T(8,128)(2,1)}) %all-gather.19.cloned.1.call-update) | async-done | bytes 1048592 | tf_op jit(solution)/shard_map/all_gather | solution.py:155
  168.9 1.5 multiply_reduce_fusion
  170.4 27.9 %all-gather.35.cloned.1.call-done = bf16[1,2048,256]{2,1,0:T(8,128)(2,1)} async-done(((bf16[1,512,256]{2,1,0:T(8,128)(2,1)}), bf16[1,2048,256]{2,1,0:T(8,128)(2,1)}) %all-gather.35.cloned.1.call-update) | async-done | bytes 1048592 | tf_op jit(solution)/shard_map/all_gather | solution.py:120
  198.3 2.2 bitcast_reduce_fusion
  200.6 3.7 %collective-permute-start.7 = (bf16[256,256]{0,1:T(8,128)(2,1)S(1)}, bf16[256,256]{0,1:T(8,128)(2,1)S(1)}, u32[]{:S(2)}, u32[]{:S(2)}) collective-permute-start(bf16[256,256]{0,1:T(8,128)(2,1)S(1)} %fusion.59), channel_id=1, source_target_pairs={{0,8},{4,12},{1,9},{5,13},{2,10},{6,14},{3,11},{7,15},{16,24},{20,... | collective-permute-start | bytes 393224 | tf_op jit(solution)/shard_map/ppermute | solution.py:18
  204.4 3.1 collective-permute-start.8
  207.7 19.0 %all-gather.31.cloned.1.call-done = bf16[1,2048,256]{2,1,0:T(8,128)(2,1)} async-done(((bf16[1,512,256]{2,1,0:T(8,128)(2,1)}), bf16[1,2048,256]{2,1,0:T(8,128)(2,1)}) %all-gather.31.cloned.1.call-update) | async-done | bytes 1048592 | tf_op jit(solution)/shard_map/all_gather | solution.py:125
  226.7 2.4 convolution_convert_fusion
  229.1 7.3 %collective-permute-start.9 = (bf16[256,256]{1,0:T(8,128)(2,1)}, bf16[256,256]{1,0:T(8,128)(2,1)}, u32[]{:S(2)}, u32[]{:S(2)}) collective-permute-start(bf16[256,256]{1,0:T(8,128)(2,1)} %convolution_convert_fusion), channel_id=1, source_target_pairs={{0,4},{4,8},{8,12},{1,5},{5,9},{9,13},{2,6},{6,10},{10,14},{3,7},{... | collective-permute-start | bytes 393224 | tf_op jit(solution)/shard_map/ppermute | solution.py:18
  236.4 4.2 %collective-permute-start.6 = (bf16[256,256]{1,0:T(8,128)(2,1)}, bf16[256,256]{1,0:T(8,128)(2,1)}, u32[]{:S(2)}, u32[]{:S(2)}) collective-permute-start(bf16[256,256]{1,0:T(8,128)(2,1)} %convolution_convert_fusion), channel_id=1, source_target_pairs={{0,8},{4,12},{1,9},{5,13},{2,10},{6,14},{3,11},{7,15},{16,24},{20,... | collective-permute-start | bytes 393224 | tf_op jit(solution)/shard_map/ppermute | solution.py:18
  240.6 1.8 slice.729
  242.4 18.9 %all-gather.33.cloned.1.call-done = bf16[1,2048,256]{2,1,0:T(8,128)(2,1)} async-done(((bf16[1,512,256]{2,1,0:T(8,128)(2,1)}), bf16[1,2048,256]{2,1,0:T(8,128)(2,1)}) %all-gather.33.cloned.1.call-update) | async-done | bytes 1048592 | tf_op jit(solution)/shard_map/all_gather | solution.py:115
  261.2 1.9 bitcast_reduce_fusion.1
  263.9 1.6 convert_element_type.60
  267.7 1.3 pad_maximum_fusion.1
  270.5 1.0 fusion.83
  271.7 1.0 fusion.81
  272.7 1.1 slice.700
  277.4 1.0 fusion.73
  278.4 3.6 %concatenate.98 = f32[4,4,64,576]{3,2,1,0:T(8,128)S(1)} concatenate(f32[4,4,64,64]{3,2,1,0:T(8,128)} %fusion.87, f32[4,4,64,64]{3,2,1,0:T(8,128)} %fusion.85, f32[4,4,64,64]{3,2,1,0:T(8,128)} %fusion.83, f32[4,4,64,64]{3,2,1,0:T(8,128)} %fusion.81, f32[4,4,64,64]{3,2,1,0:T(8,128)} %fusion.79, f32[4,4,64,64]{3,2,1,0:T(8,128)} %fusion.77, f32[4,4,64,64]{3,2,1,0:T(8,128)} %fusion.75, ...), dimensions={3} | concatenate | bytes 4718592 | tf_op jit(solution)/shard_map/concatenate | solution.py:56
  282.0 2.3 fusion.267
  284.4 1.1 constant_dynamic-update-slice_fusion.71
  285.5 1.8 pad_maximum_fusion
  288.3 1.1 slice.710
  291.2 1.2 slice.688
  292.4 1.3 fusion.13
  294.0 1.1 slice.716
  295.1 1.1 slice.724
  296.3 1.1 slice.718
  299.8 8.3 %all_gather.45 = bf16[256,1024]{1,0:T(8,128)(2,1)S(1)} all-gather(bf16[256,256]{1,0:T(8,128)(2,1)S(1)} %reshape.226), channel_id=1, replica_groups=mesh['grp'=2,'sp'=4,'tp'=4] {'tp'}, dimensions={1}, use_global_device_ids=true | all-gather | bytes 655360 | tf_op jit(solution)/shard_map/all_gather | solution.py:147
  308.1 2.5 fusion.17
  310.7 18.2 %all-gather.21.cloned.1.call-done = bf16[256,2048]{1,0:T(8,128)(2,1)} async-done(((bf16[256,512]{1,0:T(8,128)(2,1)}), bf16[256,2048]{1,0:T(8,128)(2,1)}) %all-gather.21.cloned.1.call-update) | async-done | bytes 1048592 | tf_op jit(solution)/shard_map/all_gather | solution.py:155
  328.9 2.3 copy.233
  (243 shorter events, 42.8 us)
Async XLA Ops:
  6.5 4.1 %copy-start.12 = (bf16[2,512,256]{2,1,0:T(8,128)(2,1)S(1)}, bf16[2,512,256]{2,1,0:T(8,128)(2,1)}, u32[]{:S(2)}) copy-start(bf16[2,512,256]{2,1,0:T(8,128)(2,1)} %param.13) | copy-start | bytes 1572868
  6.5 5.0 %copy-start.17 = (s32[256]{0:T(256)S(1)}, s32[256]{0:T(256)}, u32[]{:S(2)}) copy-start(s32[256]{0:T(256)} %param.11) | copy-start | bytes 3076
  6.5 14.5 %copy-start.13 = (bf16[2,256,512]{2,1,0:T(8,128)(2,1)S(1)}, bf16[2,256,512]{2,1,0:T(8,128)(2,1)}, u32[]{:S(2)}) copy-start(bf16[2,256,512]{2,1,0:T(8,128)(2,1)} %param.16) | copy-start | bytes 1572868
  6.5 33.1 %all-gather.27.cloned.1.call-start = ((), (), s32[]{:S(2)}) async-start(), calls=%async_computation.4 | async-start | bytes 1310720 | tf_op jit(solution)/shard_map/all_gather | solution.py:120
  8.5 13.5 %copy-start.16 = (f32[4,513]{1,0:T(4,128)S(1)}, f32[4,513]{1,0:T(4,128)}, u32[]{:S(2)}) copy-start(f32[4,513]{1,0:T(4,128)} %param.19) | copy-start | bytes 24628
  8.5 13.7 %copy-start.15 = (f32[2,2048]{1,0:T(2,128)S(1)}, f32[2,2048]{1,0:T(2,128)}, u32[]{:S(2)}) copy-start(f32[2,2048]{1,0:T(2,128)} %param.12) | copy-start | bytes 49156
  8.5 13.7 %copy-start.3 = (bf16[256,2048]{1,0:T(8,128)(2,1)S(1)}, bf16[256,2048]{1,0:T(8,128)(2,1)}, u32[]{:S(2)}) copy-start(bf16[256,2048]{1,0:T(8,128)(2,1)} %param.10) | copy-start | bytes 3145732
  8.5 60.2 %all-gather.23.cloned.1.call-start = ((), (), s32[]{:S(2)}) async-start(), calls=%async_computation.2 | async-start | bytes 1310720 | tf_op jit(solution)/shard_map/all_gather | solution.py:125
  10.5 12.0 %copy-start.18 = (f32[2,64]{1,0:T(2,128)S(1)}, f32[2,64]{1,0:T(2,128)}, u32[]{:S(2)}) copy-start(f32[2,64]{1,0:T(2,128)} %param.17) | copy-start | bytes 1540
  10.5 12.0 %copy-start.19 = (f32[2,64]{1,0:T(2,128)S(1)}, f32[2,64]{1,0:T(2,128)}, u32[]{:S(2)}) copy-start(f32[2,64]{1,0:T(2,128)} %param.18) | copy-start | bytes 1540
  10.6 90.5 %all-gather.25.cloned.1.call-start = ((), (), s32[]{:S(2)}) async-start(), calls=%async_computation.3 | async-start | bytes 1310720 | tf_op jit(solution)/shard_map/all_gather | solution.py:115
  11.5 136.6 %all-gather.29.cloned.1.call-start = ((), (), s32[]{:S(2)}) async-start(), calls=%async_computation.5 | async-start | bytes 1310720 | tf_op jit(solution)/shard_map/all_gather | solution.py:150
  11.6 18.6 %collective-permute-start.1 = (s32[256]{0:T(256)S(1)}, s32[256]{0:T(256)S(1)}, u32[]{:S(2)}, u32[]{:S(2)}) collective-permute-start(s32[256]{0:T(256)S(1)} %copy-done.17), channel_id=1, source_target_pairs={{0,8},{4,12},{1,9},{5,13},{2,10},{6,14},{3,11},{7,15},{16,24},{20,... | collective-permute-start | bytes 3080 | tf_op jit(solution)/shard_map/ppermute | solution.py:18
  17.5 12.7 %collective-permute-start.2 = (s32[256]{0:T(256)S(1)}, s32[256]{0:T(256)S(1)}, u32[]{:S(2)}, u32[]{:S(2)}) collective-permute-start(s32[256]{0:T(256)S(1)} %copy-done.17), channel_id=1, source_target_pairs={{0,4},{4,8},{8,12},{1,5},{5,9},{9,13},{2,6},{6,10},{10,14},{3,7},{... | collective-permute-start | bytes 3080 | tf_op jit(solution)/shard_map/ppermute | solution.py:18
  21.9 147.0 %all-gather.19.cloned.1.call-start = ((), (), s32[]{:S(2)}) async-start(), calls=%async_computation | async-start | bytes 1310720 | tf_op jit(solution)/shard_map/all_gather | solution.py:155
  30.6 91.7 %copy-start.5 = (pred[4,64,576]{2,1,0:T(8,128)(4,1)}, pred[4,64,576]{2,1,0:T(8,128)(4,1)S(1)}, u32[]{:S(2)}) copy-start(pred[4,64,576]{2,1,0:T(8,128)(4,1)S(1)} %compare_and_fusion) | copy-start | bytes 442372
  41.7 63.0 %collective-permute-start.3 = (bf16[256,256]{0,1:T(8,128)(2,1)S(1)}, bf16[256,256]{0,1:T(8,128)(2,1)S(1)}, u32[]{:S(2)}, u32[]{:S(2)}) collective-permute-start(bf16[256,256]{0,1:T(8,128)(2,1)S(1)} %fusion.61), channel_id=1, source_target_pairs={{0,8},{4,12},{1,9},{5,13},{2,10},{6,14},{3,11},{7,15},{16,24},{20,... | collective-permute-start | bytes 393224 | tf_op jit(solution)/shard_map/ppermute | solution.py:18
  45.4 60.5 %collective-permute-start.4 = (bf16[256,256]{0,1:T(8,128)(2,1)S(1)}, bf16[256,256]{0,1:T(8,128)(2,1)S(1)}, u32[]{:S(2)}, u32[]{:S(2)}) collective-permute-start(bf16[256,256]{0,1:T(8,128)(2,1)S(1)} %fusion.61), channel_id=1, source_target_pairs={{0,4},{4,8},{8,12},{1,5},{5,9},{9,13},{2,6},{6,10},{10,14},{3,7},{... | collective-permute-start | bytes 393224 | tf_op jit(solution)/shard_map/ppermute | solution.py:18
  70.5 44.1 %collective-permute-start.5 = (bf16[256,256]{1,0:T(8,128)(2,1)S(1)}, bf16[256,256]{1,0:T(8,128)(2,1)S(1)}, u32[]{:S(2)}, u32[]{:S(2)}) collective-permute-start(bf16[256,256]{1,0:T(8,128)(2,1)S(1)} %convolution_convert_fusion.1), channel_id=1, source_target_pairs={{0,4},{4,8},{8,12},{1,5},{5,9},{9,13},{2,6},{6,10},{10,14},{3,7},{... | collective-permute-start | bytes 393224 | tf_op jit(solution)/shard_map/ppermute | solution.py:18
  76.1 38.5 %collective-permute-start = (bf16[256,256]{1,0:T(8,128)(2,1)S(1)}, bf16[256,256]{1,0:T(8,128)(2,1)S(1)}, u32[]{:S(2)}, u32[]{:S(2)}) collective-permute-start(bf16[256,256]{1,0:T(8,128)(2,1)S(1)} %convolution_convert_fusion.1), channel_id=1, source_target_pairs={{0,8},{4,12},{1,9},{5,13},{2,10},{6,14},{3,11},{7,15},{16,24},{20,... | collective-permute-start | bytes 393224 | tf_op jit(solution)/shard_map/ppermute | solution.py:18
  114.6 3.2 copy-start.11
  114.6 3.2 copy-start.14
  123.3 1.0 copy-start.9
  123.3 1.3 copy-start.10
  137.7 1.0 copy-start.8
  150.6 47.7 %all-gather.35.cloned.1.call-start = ((), (), s32[]{:S(2)}) async-start(), calls=%async_computation.8 | async-start | bytes 1310720 | tf_op jit(solution)/shard_map/all_gather | solution.py:120
  151.2 75.5 %all-gather.31.cloned.1.call-start = ((), (), s32[]{:S(2)}) async-start(), calls=%async_computation.6 | async-start | bytes 1310720 | tf_op jit(solution)/shard_map/all_gather | solution.py:125
  152.0 109.3 %all-gather.33.cloned.1.call-start = ((), (), s32[]{:S(2)}) async-start(), calls=%async_computation.7 | async-start | bytes 1310720 | tf_op jit(solution)/shard_map/all_gather | solution.py:115
  152.7 155.4 %all-gather.37.cloned.1.call-start = ((), (), s32[]{:S(2)}) async-start(), calls=%async_computation.9 | async-start | bytes 1310720 | tf_op jit(solution)/shard_map/all_gather | solution.py:150
  153.4 175.5 %all-gather.21.cloned.1.call-start = ((), (), s32[]{:S(2)}) async-start(), calls=%async_computation.1 | async-start | bytes 1310720 | tf_op jit(solution)/shard_map/all_gather | solution.py:155
  170.4 56.3 %copy-start.4 = (bf16[256,2048]{1,0:T(8,128)(2,1)S(1)}, bf16[256,2048]{1,0:T(8,128)(2,1)}, u32[]{:S(2)}) copy-start(bf16[256,2048]{1,0:T(8,128)(2,1)} %all-gather.19.cloned.1.call-done) | copy-start | bytes 3145732
  200.6 65.9 %collective-permute-start.7 = (bf16[256,256]{0,1:T(8,128)(2,1)S(1)}, bf16[256,256]{0,1:T(8,128)(2,1)S(1)}, u32[]{:S(2)}, u32[]{:S(2)}) collective-permute-start(bf16[256,256]{0,1:T(8,128)(2,1)S(1)} %fusion.59), channel_id=1, source_target_pairs={{0,8},{4,12},{1,9},{5,13},{2,10},{6,14},{3,11},{7,15},{16,24},{20,... | collective-permute-start | bytes 393224 | tf_op jit(solution)/shard_map/ppermute | solution.py:18
  204.4 63.4 %collective-permute-start.8 = (bf16[256,256]{0,1:T(8,128)(2,1)S(1)}, bf16[256,256]{0,1:T(8,128)(2,1)}, u32[]{:S(2)}, u32[]{:S(2)}) collective-permute-start(bf16[256,256]{0,1:T(8,128)(2,1)S(1)} %fusion.59), channel_id=1, source_target_pairs={{0,4},{4,8},{8,12},{1,5},{5,9},{9,13},{2,6},{6,10},{10,14},{3,7},{... | collective-permute-start | bytes 393224 | tf_op jit(solution)/shard_map/ppermute | solution.py:18
  229.1 56.4 %collective-permute-start.9 = (bf16[256,256]{1,0:T(8,128)(2,1)}, bf16[256,256]{1,0:T(8,128)(2,1)}, u32[]{:S(2)}, u32[]{:S(2)}) collective-permute-start(bf16[256,256]{1,0:T(8,128)(2,1)} %convolution_convert_fusion), channel_id=1, source_target_pairs={{0,4},{4,8},{8,12},{1,5},{5,9},{9,13},{2,6},{6,10},{10,14},{3,7},{... | collective-permute-start | bytes 393224 | tf_op jit(solution)/shard_map/ppermute | solution.py:18
  236.4 48.0 %collective-permute-start.6 = (bf16[256,256]{1,0:T(8,128)(2,1)}, bf16[256,256]{1,0:T(8,128)(2,1)}, u32[]{:S(2)}, u32[]{:S(2)}) collective-permute-start(bf16[256,256]{1,0:T(8,128)(2,1)} %convolution_convert_fusion), channel_id=1, source_target_pairs={{0,8},{4,12},{1,9},{5,13},{2,10},{6,14},{3,11},{7,15},{16,24},{20,... | collective-permute-start | bytes 393224 | tf_op jit(solution)/shard_map/ppermute | solution.py:18
  278.4 3.6 %copy-start.6 = (pred[4,64,576]{2,1,0:T(8,128)(4,1)S(1)}, pred[4,64,576]{2,1,0:T(8,128)(4,1)}, u32[]{:S(2)}) copy-start(pred[4,64,576]{2,1,0:T(8,128)(4,1)} %copy-done.5) | copy-start | bytes 442372
  284.4 5.1 %copy-start = (f32[4,4,64,576]{3,2,1,0:T(8,128)S(1)}, f32[4,4,64,576]{3,2,1,0:T(8,128)}, u32[]{:S(2)}) copy-start(f32[4,4,64,576]{3,2,1,0:T(8,128)} %get-tuple-element.66) | copy-start | bytes 7077892
  289.7 1.1 copy-start.1
  291.2 2.5 copy-start.2
  298.1 1.0 copy-start.7
Sparse Core Ops, SparseCore 0:
  8.9 30.7 all-gather.26
  41.2 27.4 all-gather.22
  70.3 30.6 all-gather.24
  102.4 31.1 all-gather.28
  150.8 18.0 all-gather.18
  170.3 27.9 all-gather.34
  199.9 26.7 all-gather.30
  228.2 32.9 all-gather.32
  262.8 30.7 all-gather.36
  310.8 18.0 all-gather.20
where the time goes:
time: 339 us; the launch traced here: 338 us
  waiting for transfers between devices  152 us (45%)
  matrix products  46.2 us (14%)
  local copies, waits for them, and re-layouts  45.6 us (13%)
  starting transfers between devices  44.3 us (13%)
  other arithmetic  19 us (6%)
  blocking collectives  17.1 us (5%)
  between operations  14.4 us (4%)
    ppermute x10, starting transfers between devices, shifted(): lax.ppermute(value, axis, [(source, source + steps) for source in range(i...  43.9 us
    all_gather x2, waiting for transfers between devices, on_device(): lax.all_gather(value_weight[layer], 'sp', axis=0, tiled=True)  39.8 us
    all_gather x2, waiting for transfers between devices, on_device(): lax.all_gather(query_weight[layer], 'sp', axis=0, tiled=True)  38.6 us
    all_gather x2, waiting for transfers between devices, on_device(): lax.all_gather(key_weight[layer], 'sp', axis=0, tiled=True)  37 us
    all_gather x2, waiting for transfers between devices, on_device(): x = lax.all_gather(new_cols, 'tp', axis=1, tiled=True)  33.5 us
    slice x20, local copies, waits for them, and re-layouts, attend(): value_blocks[earlier:earlier + count]  20.2 us
    dot_general x18, matrix products, attend(): jnp.einsum('nqhd,nkhd->nhqk', blocks, key_blocks[earlier:earlier + count]...  18.4 us
    all_gather x2, blocking collectives, on_device(): all_heads = lax.all_gather(attended, 'tp', axis=1, tiled=True)  17.1 us
  transfers between devices with their start and end apart: 20, of which 8 were waited for; matrix products, arithmetic and copies ran while one was open for 29% of the time, Pallas kernels for 0%

commit v1 on v0

--- a/solution.py
+++ b/solution.py
@@ -1,6 +1,10 @@
+import functools
+
 import jax
 import jax.numpy as jnp
 from jax import lax
+from jax.experimental import pallas as pl
+from jax.experimental.pallas import tpu as pltpu
 from jax.sharding import PartitionSpec as P
 
 SEG = 64
@@ -156,6 +160,430 @@
     return x
 
 
+MESH = pl.DeviceIdType.MESH
+NEG = -1e30
+
+
+def fused_kernel(
+    sizes,
+    x_ref,
+    docs_ref,
+    ngain_ref,
+    wt_ref,
+    woin_ref,
+    qgain_ref,
+    kgain_ref,
+    frow_ref,
+    out_ref,
+    xg,
+    wq,
+    wo,
+    docs,
+    dcol,
+    ag,
+    fin,
+    bias,
+    nb,
+    q_s,
+    k_s,
+    v_s,
+    o_s,
+    doc_send,
+    doc_recv,
+    xz_send,
+    xz_recv,
+    xa_send,
+    xa_recv,
+    xb_send,
+    xb_recv,
+    xc_send,
+    xc_recv,
+    wz_send,
+    wz_recv,
+    wy_send,
+    wy_recv,
+    oz_send,
+    oz_recv,
+    oy_send,
+    oy_recv,
+    az_send,
+    az_recv,
+    at_send,
+    at_recv,
+    fn_send,
+    fn_recv,
+):
+    groups, seqs, tps = sizes
+    rows, width = x_ref.shape
+    cols = width // tps
+    head = qgain_ref.shape[1]
+    layers = wt_ref.shape[0]
+    depth = bias.shape[0] - 1
+    grp = lax.axis_index("grp")
+    s = lax.axis_index("sp")
+    t = lax.axis_index("tp")
+    other_grp = 1 - grp
+    core = t + 1 - 2 * lax.rem(t, 2)
+    side = lax.rem(t + 2, tps)
+    diag = core + 2 - 4 * (core // 2)
+    started = []
+
+    def send(src, dst, send_sem, recv_sem, where):
+        copy = pltpu.make_async_remote_copy(
+            src_ref=src,
+            dst_ref=dst,
+            send_sem=send_sem,
+            recv_sem=recv_sem,
+            device_id=where,
+            device_id_type=MESH,
+        )
+        copy.start()
+        started.append(copy)
+        return copy
+
+    def ahead(o):
+        return lax.rem(s + o, seqs)
+
+    def behind(o):
+        return lax.rem(s + seqs - o, seqs)
+
+    def block_rows(i):
+        return pl.ds(pl.multiple_of(i * rows, rows), rows)
+
+    barrier = pltpu.get_barrier_semaphore()
+    partners = [{"sp": ahead(o)} for o in range(1, seqs)]
+    partners += [{"tp": core}, {"tp": side}, {"grp": other_grp}]
+    for where in partners:
+        pl.semaphore_signal(barrier, inc=1, device_id=where, device_id_type=MESH)
+    pl.semaphore_wait(barrier, len(partners))
+
+    own_cols = pl.ds(pl.multiple_of(t * cols, cols), cols)
+    whalf = wt_ref.shape[2] // 2
+    ohalf = woin_ref.shape[1] // 2
+    wpart = pl.ds(pl.multiple_of(grp * whalf, whalf), whalf)
+    opart = pl.ds(pl.multiple_of(grp * ohalf, ohalf), ohalf)
+    hops = list(range(1, seqs))
+
+    doc_c = [
+        send(docs_ref, docs.at[s], doc_send.at[o], doc_recv.at[o], {"sp": ahead(o)}) for o in hops
+    ]
+    xz = {
+        o: send(
+            x_ref.at[:, own_cols],
+            xg.at[0, t, block_rows(s), :],
+            xz_send.at[0, o],
+            xz_recv.at[0, o],
+            {"sp": ahead(o)},
+        )
+        for o in hops
+    }
+
+    def send_qkv(layer):
+        return {
+            o: send(
+                wt_ref.at[layer, ahead(o), wpart, :],
+                wq.at[layer, s, wpart, :],
+                wz_send.at[layer, o],
+                wz_recv.at[layer, o],
+                {"sp": ahead(o)},
+            )
+            for o in hops
+        }
+
+    def send_out(layer):
+        return {
+            o: send(
+                woin_ref.at[layer, opart, :],
+                wo.at[layer, s, opart, :],
+                oz_send.at[layer, o],
+                oz_recv.at[layer, o],
+                {"sp": ahead(o)},
+            )
+            for o in hops
+        }
+
+    def relay_qkv(layer, flying):
+        result = []
+        for o in hops:
+            flying[o].wait_recv()
+            block = wq.at[layer, behind(o), wpart, :]
+            result.append(
+                send(block, block, wy_send.at[layer, o], wy_recv.at[layer, o], {"grp": other_grp})
+            )
+        return result
+
+    def relay_out(layer, flying):
+        result = []
+        for o in hops:
+            flying[o].wait_recv()
+            block = wo.at[layer, behind(o), opart, :]
+            result.append(
+                send(block, block, oy_send.at[layer, o], oy_recv.at[layer, o], {"grp": other_grp})
+            )
+        return result
+
+    qkv_fly = send_qkv(0)
+
+    for part in range(tps):
+        xg[0, part, block_rows(s), :] = x_ref[:, part * cols : (part + 1) * cols]
+    for layer in range(layers):
+        wq[layer, s] = wt_ref[layer, s]
+        wo[layer, s] = woin_ref[layer]
+    docs[s] = docs_ref[...]
+    key_seg = lax.broadcasted_iota(jnp.int32, (rows, rows), 0) // SEG
+    query_seg = lax.broadcasted_iota(jnp.int32, (rows, rows), 1) // SEG
+    for d in range(depth + 1):
+        spread = jnp.broadcast_to(frow_ref[d : d + 1, :], (rows, 2 * rows))
+        rolled = pltpu.roll(spread, 0, 1, stride=1, stride_axis=0)
+        gap = query_seg + (d * rows) // SEG - key_seg
+        bias[d] = jnp.where((gap >= 0) & (gap <= LEFT), rolled[:, rows:], NEG)
+    for copy in doc_c:
+        copy.wait_recv()
+    for i in range(seqs):
+        dcol[i] = jnp.transpose(jnp.broadcast_to(docs[i, 0:1, :], (128, rows)))
+
+    def spread_tp(layer, first):
+        to_core, to_side, to_diag = {}, {}, {}
+
+        def fan(o):
+            if o > 0:
+                xz[o].wait_recv()
+            block = xg.at[layer, t, block_rows(behind(o)), :]
+            to_side[o] = send(
+                block, block, xb_send.at[layer, o], xb_recv.at[layer, o], {"tp": side}
+            )
+            to_core[o] = send(
+                block, block, xa_send.at[layer, o], xa_recv.at[layer, o], {"tp": core}
+            )
+
+        def pass_on(o):
+            to_side[o].wait_recv()
+            block = xg.at[layer, side, block_rows(behind(o)), :]
+            to_diag[o] = send(
+                block, block, xc_send.at[layer, o], xc_recv.at[layer, o], {"tp": core}
+            )
+
+        order = list(range(first, seqs))
+        for place, o in enumerate(order):
+            fan(o)
+            if place >= 1:
+                pass_on(order[place - 1])
+        pass_on(order[-1])
+        return to_core, to_diag
+
+    def project(layer, o):
+        i = behind(o)
+        total = jnp.zeros((rows, 1), jnp.float32)
+        for part in range(tps):
+            piece = xg[layer, part, block_rows(i), :].astype(jnp.float32)
+            total = total + jnp.sum(piece * piece, axis=1, keepdims=True)
+        factor = lax.rsqrt(total * (1.0 / width) + epsilon)
+        for part in range(tps):
+            piece = xg[layer, part, block_rows(i), :].astype(jnp.float32)
+            gain = ngain_ref[layer : layer + 1, part * cols : (part + 1) * cols]
+            nb[:, part * cols : (part + 1) * cols] = (piece * factor * gain).astype(jnp.bfloat16)
+        span = width // seqs
+        raw = jnp.zeros((3 * head, rows), jnp.float32)
+        for part in range(seqs):
+            raw = raw + lax.dot_general(
+                wq[layer, part],
+                nb[:, part * span : (part + 1) * span],
+                (((1,), (1,)), ((), ())),
+                preferred_element_type=jnp.float32,
+            )
+
+        def normal(value, gain):
+            mean = jnp.mean(value * value, axis=0, keepdims=True)
+            return value * lax.rsqrt(mean + epsilon) * gain
+
+        q_s[i] = (normal(raw[:head], qgain_ref[layer]) * head ** (-0.5)).astype(jnp.bfloat16)
+        k_s[i] = jnp.transpose(normal(raw[head : 2 * head], kgain_ref[layer])).astype(jnp.bfloat16)
+        v_s[i] = raw[2 * head :].astype(jnp.bfloat16)
+
+    def attention():
+        for j in range(seqs):
+            pieces = []
+            for i in range(max(0, j - depth), j + 1):
+                score = jnp.dot(k_s[i], q_s[j], preferred_element_type=jnp.float32)
+                same = dcol[i][:, 0:1] == docs[j, 0:1, :]
+                pieces.append((i, jnp.where(same, score + bias[j - i], NEG)))
+            peak = pieces[0][1].max(axis=0, keepdims=True)
+            for _, piece in pieces[1:]:
+                peak = jnp.maximum(peak, piece.max(axis=0, keepdims=True))
+            mass = jnp.zeros((1, rows), jnp.float32)
+            mixed = jnp.zeros((head, rows), jnp.float32)
+            for i, piece in pieces:
+                expo = jnp.exp(piece - peak)
+                mass = mass + jnp.sum(expo, axis=0, keepdims=True)
+                mixed = mixed + jnp.dot(
+                    v_s[i], expo.astype(jnp.bfloat16), preferred_element_type=jnp.float32
+                )
+            o_s[lax.rem(j, seqs)] = (mixed / mass).astype(jnp.bfloat16)
+
+    for layer in range(layers):
+        last = layer == layers - 1
+        first = 1 if layer == 0 else 0
+        to_core, to_diag = spread_tp(layer, first)
+        if layer == 0:
+            project_ready = relay_qkv(0, qkv_fly)
+            out_fly = send_out(0)
+        for copy in project_ready:
+            copy.wait_recv()
+        if layer == 0:
+            project(layer, 0)
+        for o in range(first, seqs):
+            to_core[o].wait_recv()
+            to_diag[o].wait_recv()
+            project(layer, o)
+        if layer > 0:
+            for copy in outgoing:
+                copy.wait_send()
+            started[:] = [copy for copy in started if all(copy is not old for old in outgoing)]
+        attention()
+        outgoing = [
+            send(
+                o_s.at[ahead(o)],
+                ag.at[layer, t, s],
+                az_send.at[layer, o],
+                az_recv.at[layer, o],
+                {"sp": ahead(o)},
+            )
+            for o in hops
+        ]
+        if not last:
+            qkv_fly = send_qkv(layer + 1)
+        ag[layer, t, s] = o_s[s]
+        out_ready = relay_out(layer, out_fly)
+        for copy in outgoing:
+            copy.wait_recv()
+        block = ag.at[layer, t]
+        across = send(block, block, at_send.at[layer, 0], at_recv.at[layer, 0], {"tp": side})
+        beside = send(block, block, at_send.at[layer, 1], at_recv.at[layer, 1], {"tp": core})
+        across.wait_recv()
+        block = ag.at[layer, side]
+        corner = send(block, block, at_send.at[layer, 2], at_recv.at[layer, 2], {"tp": core})
+        for copy in out_ready:
+            copy.wait_recv()
+        beside.wait_recv()
+        corner.wait_recv()
+        heads_all = ag[layer].reshape(tps * seqs * head, rows)
+        weight = wo[layer].reshape(-1, cols)
+        product = lax.dot_general(
+            heads_all,
+            weight,
+            (((0,), (0,)), ((), ())),
+            preferred_element_type=jnp.float32,
+        )
+        kept = xg[layer, t, block_rows(s), :].astype(jnp.float32)
+        fresh = (kept + product).astype(jnp.bfloat16)
+        if not last:
+            xg[layer + 1, t, block_rows(s), :] = fresh
+            mine = xg.at[layer + 1, t, block_rows(s), :]
+            xz = {
+                o: send(
+                    mine,
+                    mine,
+                    xz_send.at[layer + 1, o],
+                    xz_recv.at[layer + 1, o],
+                    {"sp": ahead(o)},
+                )
+                for o in hops
+            }
+            project_ready = relay_qkv(layer + 1, qkv_fly)
+            out_fly = send_out(layer + 1)
+        else:
+            fin[t] = fresh
+            cuts = fn_send.shape[0]
+            tall = rows // cuts
+            crossing, beside = [], []
+            for c in range(cuts):
+                part = fin.at[t, pl.ds(c * tall, tall), :]
+                crossing.append(send(part, part, fn_send.at[c, 0], fn_recv.at[c, 0], {"tp": side}))
+                beside.append(send(part, part, fn_send.at[c, 1], fn_recv.at[c, 1], {"tp": core}))
+            for c in range(cuts):
+                crossing[c].wait_recv()
+                part = fin.at[side, pl.ds(c * tall, tall), :]
+                beside.append(send(part, part, fn_send.at[c, 2], fn_recv.at[c, 2], {"tp": core}))
+            for copy in beside:
+                copy.wait_recv()
+            for part in range(tps):
+                out_ref[:, part * cols : (part + 1) * cols] = fin[part]
+    for copy in started:
+        copy.wait_send()
+
+
+def fused_device(
+    sizes,
+    stream,
+    doc_ids,
+    norm_gain,
+    query_weight,
+    key_weight,
+    value_weight,
+    out_weight,
+    query_gain,
+    key_gain,
+    rel_bias,
+):
+    groups, seqs, tps = sizes
+    rows, width = stream.shape
+    cols = width // tps
+    layers, deep, _ = query_weight.shape
+    head = query_gain.shape[1]
+    depth = -(-LEFT * SEG // rows)
+
+    def turned(weight):
+        return weight.reshape(layers, deep, seqs, head).transpose(0, 2, 3, 1)
+
+    wt = jnp.concatenate(
+        [turned(query_weight), turned(key_weight), turned(value_weight)], axis=2
+    )
+    row = lax.dynamic_index_in_dim(rel_bias, lax.axis_index("sp"), 0, keepdims=False)
+    span = (depth + 2) * rows
+    line = jnp.concatenate([row, jnp.broadcast_to(row[-1:], (span - row.shape[0],))])
+    frow = jnp.stack([line[d * rows : (d + 2) * rows] for d in range(depth + 1)])
+    docs8 = jnp.broadcast_to(doc_ids.astype(jnp.float32)[None], (8, rows))
+    dma = pltpu.SemaphoreType.DMA
+    bf16 = jnp.bfloat16
+    scratch = [
+        pltpu.VMEM((layers, tps, seqs * rows, cols), bf16),
+        pltpu.VMEM((layers, seqs, 3 * head, deep), bf16),
+        pltpu.VMEM((layers, seqs) + out_weight.shape[1:], bf16),
+        pltpu.VMEM((seqs, 8, rows), jnp.float32),
+        pltpu.VMEM((seqs, rows, 128), jnp.float32),
+        pltpu.VMEM((layers, tps, seqs, head, rows), bf16),
+        pltpu.VMEM((tps, rows, cols), bf16),
+        pltpu.VMEM((depth + 1, rows, rows), jnp.float32),
+        pltpu.VMEM((rows, width), bf16),
+        pltpu.VMEM((seqs, head, rows), bf16),
+        pltpu.VMEM((seqs, rows, head), bf16),
+        pltpu.VMEM((seqs, head, rows), bf16),
+        pltpu.VMEM((seqs, head, rows), bf16),
+    ]
+    scratch += [dma((seqs,))] * 2 + [dma((layers, seqs))] * 16
+    scratch += [dma((layers, seqs))] * 2 + [dma((layers, 3))] * 2 + [dma((2, 3))] * 2
+    return pl.pallas_call(
+        functools.partial(fused_kernel, sizes),
+        name="fused_layers",
+        out_shape=jax.ShapeDtypeStruct((rows, width), bf16),
+        in_specs=[pl.BlockSpec(memory_space=pltpu.VMEM)] * 8,
+        out_specs=pl.BlockSpec(memory_space=pltpu.VMEM),
+        scratch_shapes=scratch,
+        compiler_params=pltpu.CompilerParams(
+            collective_id=0, has_side_effects=True, vmem_limit_bytes=60 * 1024 * 1024
+        ),
+    )(
+        stream,
+        docs8,
+        norm_gain,
+        wt,
+        out_weight,
+        query_gain[..., None],
+        key_gain[..., None],
+        frow,
+    )
+
+
 def solution(mesh):
     placed = (
         P(("grp", "sp"), None),
@@ -169,6 +597,15 @@
         P(),
         P("tp", None),
     )
+    sizes = tuple(mesh.shape[axis] for axis in ("grp", "sp", "tp"))
+
+    def body(*args):
+        one_head_each = args[-1].shape[0] == sizes[1]
+        fits = sizes[0] == 2 and sizes[2] == 4 and args[0].shape[0] == MAXREL
+        if one_head_each and fits:
+            return fused_device(sizes, *args)
+        return on_device(*args)
+
     return jax.shard_map(
-        on_device, mesh=mesh, in_specs=placed, out_specs=P(("grp", "sp"), None), check_vma=False
+        body, mesh=mesh, in_specs=placed, out_specs=P(("grp", "sp"), None), check_vma=False
     )

time: 339 us -> 152 us (0.45)
  waiting for transfers between devices: 152 us -> 0 us
  Pallas kernels: 0 us -> 139 us
  matrix products: 46.2 us -> 0 us
  starting transfers between devices: 44.3 us -> 0 us
  local copies, waits for them, and re-layouts: 45.6 us -> 10.5 us
  blocking collectives: 17.1 us -> 0 us
  other arithmetic: 19 us -> 1.95 us
  between operations: 14.4 us -> 0.07 us
    all_gather x10 -> x0, waiting for transfers between devices: 149 us -> none  [the longest x2 39.8 us: on_device(): lax.all_gather(value_weight[layer], 'sp', axis=0, tiled=True)]
    pallas_call x0 -> x1, Pallas kernels: none -> 139 us  [fused_device(): pl.pallas_call(functools.partial(fused_kernel, sizes), name='fused_layers...]
    dot_general x44 -> x0, matrix products: 46.2 us -> none  [the longest x18 18.4 us: attend(): jnp.einsum('nqhd,nkhd->nhqk', blocks, key_blocks[earlier:earlier + count]...]
    ppermute x10 -> x0, starting transfers between devices: 43.9 us -> none  [shifted(): lax.ppermute(value, axis, [(source, source + steps) for source in range(i...]
    slice x48 -> x3, local copies, waits for them, and re-layouts: 30 us -> 2.63 us  [the longest x2 1.36 us: fused_device(): frow = jnp.stack([line[d * rows:(d + 2) * rows] for d in range(depth + 1)])]
    all_gather x2 -> x0, blocking collectives: 17.1 us -> none  [on_device(): all_heads = lax.all_gather(attended, 'tp', axis=1, tiled=True)]
    concatenate x6 -> x0, local copies, waits for them, and re-layouts: 7.55 us -> none  [the longest x2 7.21 us: attend(): scores = jnp.concatenate(score_parts, axis=-1)]
    unnamed x63 -> x0, other arithmetic: 5.16 us -> none
  transfers between devices with their start and end apart: 20 -> 0, of which waited for: 8 -> 0; matrix products, arithmetic and copies ran while one was open for 29% -> 0% of each run, Pallas kernels for 0% -> 0%
where the time goes in v1:
time: 152 us; the launch traced here: 151 us
  Pallas kernels  139 us (91%)
  local copies, waits for them, and re-layouts  10.5 us (7%)
  other arithmetic  1.95 us (1%)
    pallas_call x1, Pallas kernels, fused_device(): pl.pallas_call(functools.partial(fused_kernel, sizes), name='fused_layers...  139 us
    unnamed x12, local copies, waits for them, and re-layouts  5.04 us

profile of v1, /device:TPU:0, one launch (start us, length us, event | category | flops | bytes accessed | tf_op | source)
XLA Modules:
  0.0 151.4 jit_solution(14367649965070377717)
XLA Ops:
  0.0 0.0 copy-start
  0.0 0.8 dynamic-slice_reduce_fusion
  0.8 1.3 dynamic-slice.1
  2.1 0.6 pad_slice_fusion.1
  2.7 0.7 constant_dynamic-slice_fusion
  3.4 0.6 pad_maximum_fusion.1.frow_ref
  4.0 1.3 copy.11
  5.3 1.3 copy.12
  6.5 0.0 copy-done
  6.5 0.2 copy.13
  6.8 0.0 copy-start.1
  6.8 0.0 copy-start.2
  6.8 0.0 copy-start.3
  6.8 1.3 pad_maximum_fusion.wt_ref
  8.1 0.0 copy-done.1
  8.1 0.7 copy.14.qgain_ref
  8.9 0.0 copy-done.2
  8.9 0.7 copy.15.kgain_ref
  9.6 0.0 copy-done.3
  9.6 0.6 broadcast_in_dim.8.docs_ref
  10.2 138.8 %fused_layers.1 = bf16[256,2048]{1,0:T(8,128)(2,1)} custom-call(bf16[256,2048]{1,0:T(8,128)(2,1)} %x_ref.1, f32[8,256]{1,0:T(8,128)} %broadcast_in_dim.8.docs_ref, f32[2,2048]{1,0:T(2,128)} %ngain_ref.1, bf16[2,4,192,512]{3,2,1,0:T(8,128)(2,1)} %pad_maximum_fusion.wt_ref, bf16[2,256,512]{2,1,0:T(8,128)(2,1)} %woin_ref.1, f32[2,64,1]{2,1,0:T(8,128)} %copy.14.qgain_ref, ...), custom_call_target="tpu_custom_call" | custom-call | tf_op jit(solution)/shard_map/fused_layers/pallas_call | solution.py:565
  149.1 2.3 %copy.17 = bf16[256,2048]{1,0:T(8,128)(2,1)} copy(bf16[256,2048]{1,0:T(8,128)(2,1)} %fused_layers.1) | data formatting | bytes 2097152
  (1 shorter events, 0.0 us)
Async XLA Ops:
  0.0 6.5 %copy-start = (bf16[2,512,256]{2,1,0:T(8,128)(2,1)S(1)}, bf16[2,512,256]{2,1,0:T(8,128)(2,1)}, u32[]{:S(2)}) copy-start(bf16[2,512,256]{2,1,0:T(8,128)(2,1)} %param.15) | copy-start | bytes 1572868
  6.8 1.4 copy-start.1
  6.8 2.1 %copy-start.2 = (f32[2,64]{1,0:T(2,128)S(1)}, f32[2,64]{1,0:T(2,128)}, u32[]{:S(2)}) copy-start(f32[2,64]{1,0:T(2,128)} %param.18) | copy-start | bytes 1540
  6.8 2.8 %copy-start.3 = (s32[256]{0:T(256)S(1)}, s32[256]{0:T(256)}, u32[]{:S(2)}) copy-start(s32[256]{0:T(256)} %param.11) | copy-start | bytes 3076

commit v2 on v1

--- a/solution.py
+++ b/solution.py
@@ -169,12 +169,15 @@
     x_ref,
     docs_ref,
     ngain_ref,
-    wt_ref,
+    qw_ref,
+    kw_ref,
+    vw_ref,
     woin_ref,
     qgain_ref,
     kgain_ref,
-    frow_ref,
+    bias_ref,
     out_ref,
+    wt_ref,
     xg,
     wq,
     wo,
@@ -267,16 +270,49 @@
     doc_c = [
         send(docs_ref, docs.at[s], doc_send.at[o], doc_recv.at[o], {"sp": ahead(o)}) for o in hops
     ]
-    xz = {
-        o: send(
-            x_ref.at[:, own_cols],
-            xg.at[0, t, block_rows(s), :],
-            xz_send.at[0, o],
-            xz_recv.at[0, o],
-            {"sp": ahead(o)},
-        )
-        for o in hops
-    }
+    def passing(layer, way, k, arriving):
+        block = s - k if way == 0 else s + k
+        if arriving:
+            block = block - 1 if way == 0 else block + 1
+        inside = block >= 0 if way == 0 else block < seqs
+        return block, inside
+
+    def onward(layer, way, k):
+        block, inside = passing(layer, way, k, False)
+        open_end = s < seqs - 1 if way == 0 else s > 0
+        place = xg.at[layer, t, block_rows(block), :]
+        copy = pltpu.make_async_remote_copy(
+            src_ref=x_ref.at[:, own_cols] if layer == 0 and k == 0 else place,
+            dst_ref=place,
+            send_sem=xz_send.at[layer, way, k],
+            recv_sem=xz_recv.at[layer, way, k],
+            device_id={"sp": s + 1 if way == 0 else s - 1},
+            device_id_type=MESH,
+        )
+        return copy, inside & open_end
+
+    def start_onward(layer, way, k):
+        copy, valid = onward(layer, way, k)
+
+        @pl.when(valid)
+        def _():
+            copy.start()
+
+    def tp_copy(layer, kind, block):
+        held = side if kind == 2 else t
+        place = xg.at[layer, held, block_rows(block), :]
+        send_sem, recv_sem = ((xa_send, xa_recv), (xb_send, xb_recv), (xc_send, xc_recv))[kind]
+        return pltpu.make_async_remote_copy(
+            src_ref=place,
+            dst_ref=place,
+            send_sem=send_sem.at[layer, block],
+            recv_sem=recv_sem.at[layer, block],
+            device_id={"tp": side if kind == 1 else core},
+            device_id_type=MESH,
+        )
+
+    for way in (0, 1):
+        start_onward(0, way, 0)
 
     def send_qkv(layer):
         return {
@@ -322,18 +358,25 @@
             )
         return result
 
-    qkv_fly = send_qkv(0)
-
     for part in range(tps):
         xg[0, part, block_rows(s), :] = x_ref[:, part * cols : (part + 1) * cols]
     for layer in range(layers):
+        for which, source in enumerate((qw_ref, kw_ref, vw_ref)):
+            turned = jnp.transpose(source[layer])
+            for i in range(seqs):
+                wt_ref[layer, i, which * head : (which + 1) * head, :] = turned[
+                    i * head : (i + 1) * head, :
+                ]
+        wo[layer, s] = woin_ref[layer]
         wq[layer, s] = wt_ref[layer, s]
-        wo[layer, s] = woin_ref[layer]
     docs[s] = docs_ref[...]
+    qkv_fly = send_qkv(0)
     key_seg = lax.broadcasted_iota(jnp.int32, (rows, rows), 0) // SEG
     query_seg = lax.broadcasted_iota(jnp.int32, (rows, rows), 1) // SEG
     for d in range(depth + 1):
-        spread = jnp.broadcast_to(frow_ref[d : d + 1, :], (rows, 2 * rows))
+        spread = jnp.broadcast_to(
+            bias_ref[pl.ds(s, 1), d * rows : (d + 2) * rows], (rows, 2 * rows)
+        )
         rolled = pltpu.roll(spread, 0, 1, stride=1, stride_axis=0)
         gap = query_seg + (d * rows) // SEG - key_seg
         bias[d] = jnp.where((gap >= 0) & (gap <= LEFT), rolled[:, rows:], NEG)
@@ -342,37 +385,54 @@
     for i in range(seqs):
         dcol[i] = jnp.transpose(jnp.broadcast_to(docs[i, 0:1, :], (128, rows)))
 
-    def spread_tp(layer, first):
-        to_core, to_side, to_diag = {}, {}, {}
-
-        def fan(o):
-            if o > 0:
-                xz[o].wait_recv()
-            block = xg.at[layer, t, block_rows(behind(o)), :]
-            to_side[o] = send(
-                block, block, xb_send.at[layer, o], xb_recv.at[layer, o], {"tp": side}
-            )
-            to_core[o] = send(
-                block, block, xa_send.at[layer, o], xa_recv.at[layer, o], {"tp": core}
-            )
-
-        def pass_on(o):
-            to_side[o].wait_recv()
-            block = xg.at[layer, side, block_rows(behind(o)), :]
-            to_diag[o] = send(
-                block, block, xc_send.at[layer, o], xc_recv.at[layer, o], {"tp": core}
-            )
-
-        order = list(range(first, seqs))
-        for place, o in enumerate(order):
-            fan(o)
-            if place >= 1:
-                pass_on(order[place - 1])
-        pass_on(order[-1])
-        return to_core, to_diag
-
-    def project(layer, o):
-        i = behind(o)
+    def fan(layer, block):
+        tp_copy(layer, 1, block).start()
+        tp_copy(layer, 0, block).start()
+
+    def pass_on(layer, block):
+        tp_copy(layer, 1, block).wait_recv()
+        tp_copy(layer, 2, block).start()
+
+    def spread_tp(layer, own_too):
+        if own_too:
+            fan(layer, s)
+        for k in range(seqs - 1):
+            for way in (0, 1):
+                block, inside = passing(layer, way, k, True)
+
+                @pl.when(inside)
+                def _(block=block, way=way, k=k):
+                    onward(layer, way, k)[0].wait_recv()
+                    if k + 1 < seqs - 1:
+                        start_onward(layer, way, k + 1)
+                    fan(layer, block)
+
+            if k == 0 and own_too:
+                pass_on(layer, s)
+            pass_slots(layer, k - 1)
+        pass_slots(layer, seqs - 2)
+
+    def pass_slots(layer, k):
+        if k < 0:
+            return
+        for way in (0, 1):
+            block, inside = passing(layer, way, k, True)
+
+            @pl.when(inside)
+            def _(block=block):
+                pass_on(layer, block)
+
+    def nth(v):
+        orders = [
+            sorted((b for b in range(seqs) if b != c), key=lambda b: abs(b - c))
+            for c in range(seqs)
+        ]
+        block = orders[0][v - 1]
+        for c in range(1, seqs):
+            block = jnp.where(s == c, orders[c][v - 1], block)
+        return block
+
+    def project(layer, i):
         total = jnp.zeros((rows, 1), jnp.float32)
         for part in range(tps):
             piece = xg[layer, part, block_rows(i), :].astype(jnp.float32)
@@ -394,10 +454,11 @@
 
         def normal(value, gain):
             mean = jnp.mean(value * value, axis=0, keepdims=True)
-            return value * lax.rsqrt(mean + epsilon) * gain
-
-        q_s[i] = (normal(raw[:head], qgain_ref[layer]) * head ** (-0.5)).astype(jnp.bfloat16)
-        k_s[i] = jnp.transpose(normal(raw[head : 2 * head], kgain_ref[layer])).astype(jnp.bfloat16)
+            column = jnp.transpose(jnp.broadcast_to(gain, (128, head)))[:, 0:1]
+            return value * lax.rsqrt(mean + epsilon) * column
+
+        q_s[i] = (normal(raw[:head], qgain_ref[layer : layer + 1, :]) * head ** (-0.5)).astype(jnp.bfloat16)
+        k_s[i] = jnp.transpose(normal(raw[head : 2 * head], kgain_ref[layer : layer + 1, :])).astype(jnp.bfloat16)
         v_s[i] = raw[2 * head :].astype(jnp.bfloat16)
 
     def attention():
@@ -422,19 +483,18 @@
 
     for layer in range(layers):
         last = layer == layers - 1
-        first = 1 if layer == 0 else 0
-        to_core, to_diag = spread_tp(layer, first)
+        spread_tp(layer, layer > 0)
         if layer == 0:
             project_ready = relay_qkv(0, qkv_fly)
             out_fly = send_out(0)
         for copy in project_ready:
             copy.wait_recv()
-        if layer == 0:
-            project(layer, 0)
-        for o in range(first, seqs):
-            to_core[o].wait_recv()
-            to_diag[o].wait_recv()
-            project(layer, o)
+        for v in range(seqs):
+            block = nth(v) if v else s
+            if v or layer > 0:
+                tp_copy(layer, 0, block).wait_recv()
+                tp_copy(layer, 2, block).wait_recv()
+            project(layer, block)
         if layer > 0:
             for copy in outgoing:
                 copy.wait_send()
@@ -478,17 +538,8 @@
         fresh = (kept + product).astype(jnp.bfloat16)
         if not last:
             xg[layer + 1, t, block_rows(s), :] = fresh
-            mine = xg.at[layer + 1, t, block_rows(s), :]
-            xz = {
-                o: send(
-                    mine,
-                    mine,
-                    xz_send.at[layer + 1, o],
-                    xz_recv.at[layer + 1, o],
-                    {"sp": ahead(o)},
-                )
-                for o in hops
-            }
+            for way in (0, 1):
+                start_onward(layer + 1, way, 0)
             project_ready = relay_qkv(layer + 1, qkv_fly)
             out_fly = send_out(layer + 1)
         else:
@@ -510,6 +561,17 @@
                 out_ref[:, part * cols : (part + 1) * cols] = fin[part]
     for copy in started:
         copy.wait_send()
+    for layer in range(layers):
+        for o in range(1 if layer == 0 else 0, seqs):
+            for kind in range(3):
+                tp_copy(layer, kind, ahead(o)).wait_send()
+        for way in (0, 1):
+            for k in range(seqs - 1):
+                copy, valid = onward(layer, way, k)
+
+                @pl.when(valid)
+                def _(copy=copy):
+                    copy.wait_send()
 
 
 def fused_device(
@@ -532,20 +594,14 @@
     head = query_gain.shape[1]
     depth = -(-LEFT * SEG // rows)
 
-    def turned(weight):
-        return weight.reshape(layers, deep, seqs, head).transpose(0, 2, 3, 1)
-
-    wt = jnp.concatenate(
-        [turned(query_weight), turned(key_weight), turned(value_weight)], axis=2
+    padded = jnp.pad(
+        rel_bias, ((0, 0), (0, (depth + 2) * rows - rel_bias.shape[1])), mode="edge"
     )
-    row = lax.dynamic_index_in_dim(rel_bias, lax.axis_index("sp"), 0, keepdims=False)
-    span = (depth + 2) * rows
-    line = jnp.concatenate([row, jnp.broadcast_to(row[-1:], (span - row.shape[0],))])
-    frow = jnp.stack([line[d * rows : (d + 2) * rows] for d in range(depth + 1)])
     docs8 = jnp.broadcast_to(doc_ids.astype(jnp.float32)[None], (8, rows))
     dma = pltpu.SemaphoreType.DMA
     bf16 = jnp.bfloat16
     scratch = [
+        pltpu.VMEM((layers, seqs, 3 * head, deep), bf16),
         pltpu.VMEM((layers, tps, seqs * rows, cols), bf16),
         pltpu.VMEM((layers, seqs, 3 * head, deep), bf16),
         pltpu.VMEM((layers, seqs) + out_weight.shape[1:], bf16),
@@ -560,13 +616,13 @@
         pltpu.VMEM((seqs, head, rows), bf16),
         pltpu.VMEM((seqs, head, rows), bf16),
     ]
-    scratch += [dma((seqs,))] * 2 + [dma((layers, seqs))] * 16
+    scratch += [dma((seqs,))] * 2 + [dma((layers, 2, seqs))] * 2 + [dma((layers, seqs))] * 14
     scratch += [dma((layers, seqs))] * 2 + [dma((layers, 3))] * 2 + [dma((2, 3))] * 2
     return pl.pallas_call(
         functools.partial(fused_kernel, sizes),
         name="fused_layers",
         out_shape=jax.ShapeDtypeStruct((rows, width), bf16),
-        in_specs=[pl.BlockSpec(memory_space=pltpu.VMEM)] * 8,
+        in_specs=[pl.BlockSpec(memory_space=pltpu.VMEM)] * 10,
         out_specs=pl.BlockSpec(memory_space=pltpu.VMEM),
         scratch_shapes=scratch,
         compiler_params=pltpu.CompilerParams(
@@ -576,11 +632,13 @@
         stream,
         docs8,
         norm_gain,
-        wt,
+        query_weight,
+        key_weight,
+        value_weight,
         out_weight,
-        query_gain[..., None],
-        key_gain[..., None],
-        frow,
+        query_gain,
+        key_gain,
+        padded,
     )
 
 

time: 152 us -> 133 us (0.88)
  Pallas kernels: 139 us -> 129 us
  local copies, waits for them, and re-layouts: 10.5 us -> 3.8 us
    pallas_call x1, Pallas kernels: 139 us -> 129 us  [fused_device(): pl.pallas_call(functools.partial(fused_kernel, sizes), name='fused_layers...]
    unnamed x12 -> x5, local copies, waits for them, and re-layouts: 5.04 us -> 2.33 us
    slice x3 -> x1, local copies, waits for them, and re-layouts: 2.63 us -> 0.81 us  [fused_device(): jnp.pad(rel_bias, ((0, 0), (0, (depth + 2) * rows - rel_bias.shape[1])),...]
where the time goes in v2:
time: 133 us
  Pallas kernels  129 us (97%)
  local copies, waits for them, and re-layouts  3.8 us (3%)
    pallas_call x1, Pallas kernels, fused_device(): pl.pallas_call(functools.partial(fused_kernel, sizes), name='fused_layers...  129 us

profile of v2, /device:TPU:0, one launch (start us, length us, event | category | flops | bytes accessed | tf_op | source)
XLA Modules:
  0.0 133.2 jit_solution(3075745591691977038)
XLA Ops:
  0.0 0.0 copy-start.1
  0.0 0.8 slice_reduce_fusion
  0.8 0.0 copy-done.1
  0.8 0.0 copy-start
  0.8 0.6 broadcast_in_dim.4.docs_ref
  1.4 0.1 reshape.6
  1.5 0.0 copy-done
  1.5 0.7 pad_maximum_fusion.bias_ref
  2.2 128.7 %fused_layers.1 = bf16[256,2048]{1,0:T(8,128)(2,1)} custom-call(bf16[256,2048]{1,0:T(8,128)(2,1)} %x_ref.1, f32[8,256]{1,0:T(8,128)} %broadcast_in_dim.4.docs_ref, f32[2,2048]{1,0:T(2,128)} %ngain_ref.1, bf16[2,512,256]{2,1,0:T(8,128)(2,1)} %qw_ref.1, bf16[2,512,256]{2,1,0:T(8,128)(2,1)} %kw_ref.1, bf16[2,512,256]{2,1,0:T(8,128)(2,1)} %vw_ref.1, ...), custom_call_target="tpu_custom_call" | custom-call | tf_op jit(solution)/shard_map/fused_layers/pallas_call | solution.py:621
  130.9 2.3 %copy.12 = bf16[256,2048]{1,0:T(8,128)(2,1)} copy(bf16[256,2048]{1,0:T(8,128)(2,1)} %fused_layers.1) | data formatting | bytes 2097152
  (1 shorter events, 0.0 us)
Async XLA Ops:
  0.0 0.8 copy-start.1
  0.8 0.7 copy-start

commit v3 on v2

--- a/solution.py
+++ b/solution.py
@@ -370,7 +370,6 @@
         wo[layer, s] = woin_ref[layer]
         wq[layer, s] = wt_ref[layer, s]
     docs[s] = docs_ref[...]
-    qkv_fly = send_qkv(0)
     key_seg = lax.broadcasted_iota(jnp.int32, (rows, rows), 0) // SEG
     query_seg = lax.broadcasted_iota(jnp.int32, (rows, rows), 1) // SEG
     for d in range(depth + 1):
@@ -394,6 +393,7 @@
         tp_copy(layer, 2, block).start()
 
     def spread_tp(layer, own_too):
+        fetched = None
         if own_too:
             fan(layer, s)
         for k in range(seqs - 1):
@@ -408,9 +408,19 @@
                     fan(layer, block)
 
             if k == 0 and own_too:
+                fetched = relay_qkv(layer, qkv_fly)
                 pass_on(layer, s)
+            if k == min(1, seqs - 2) and not own_too:
+                flying = send_qkv(layer)
             pass_slots(layer, k - 1)
+        out_flying = None
+        if own_too:
+            out_flying = send_out(layer)
         pass_slots(layer, seqs - 2)
+        if not own_too:
+            fetched = relay_qkv(layer, flying)
+            out_flying = send_out(layer)
+        return fetched, out_flying
 
     def pass_slots(layer, k):
         if k < 0:
@@ -483,10 +493,7 @@
 
     for layer in range(layers):
         last = layer == layers - 1
-        spread_tp(layer, layer > 0)
-        if layer == 0:
-            project_ready = relay_qkv(0, qkv_fly)
-            out_fly = send_out(0)
+        project_ready, out_fly = spread_tp(layer, layer > 0)
         for copy in project_ready:
             copy.wait_recv()
         for v in range(seqs):
@@ -540,8 +547,6 @@
             xg[layer + 1, t, block_rows(s), :] = fresh
             for way in (0, 1):
                 start_onward(layer + 1, way, 0)
-            project_ready = relay_qkv(layer + 1, qkv_fly)
-            out_fly = send_out(layer + 1)
         else:
             fin[t] = fresh
             cuts = fn_send.shape[0]

time: 133 us -> 120 us (0.902)
  Pallas kernels: 129 us -> 116 us
    pallas_call x1, Pallas kernels: 129 us -> 116 us  [fused_device(): pl.pallas_call(functools.partial(fused_kernel, sizes), name='fused_layers...]
where the time goes in v3:
time: 120 us
  Pallas kernels  116 us (97%)
  local copies, waits for them, and re-layouts  3.8 us (3%)
    pallas_call x1, Pallas kernels, fused_device(): pl.pallas_call(functools.partial(fused_kernel, sizes), name='fused_layers...  116 us

profile of v3, /device:TPU:0, one launch (start us, length us, event | category | flops | bytes accessed | tf_op | source)
XLA Modules:
  0.0 120.2 jit_solution(17652810274793033667)
XLA Ops:
  0.0 0.0 copy-start.1
  0.0 0.8 slice_reduce_fusion
  0.8 0.0 copy-done.1
  0.8 0.0 copy-start
  0.8 0.6 broadcast_in_dim.4.docs_ref
  1.4 0.1 reshape.6
  1.5 0.0 copy-done
  1.5 0.7 pad_maximum_fusion.bias_ref
  2.2 115.7 %fused_layers.1 = bf16[256,2048]{1,0:T(8,128)(2,1)} custom-call(bf16[256,2048]{1,0:T(8,128)(2,1)} %x_ref.1, f32[8,256]{1,0:T(8,128)} %broadcast_in_dim.4.docs_ref, f32[2,2048]{1,0:T(2,128)} %ngain_ref.1, bf16[2,512,256]{2,1,0:T(8,128)(2,1)} %qw_ref.1, bf16[2,512,256]{2,1,0:T(8,128)(2,1)} %kw_ref.1, bf16[2,512,256]{2,1,0:T(8,128)(2,1)} %vw_ref.1, ...), custom_call_target="tpu_custom_call" | custom-call | tf_op jit(solution)/shard_map/fused_layers/pallas_call | solution.py:626
  117.9 2.3 %copy.12 = bf16[256,2048]{1,0:T(8,128)(2,1)} copy(bf16[256,2048]{1,0:T(8,128)(2,1)} %fused_layers.1) | data formatting | bytes 2097152
  (1 shorter events, 0.0 us)
Async XLA Ops:
  0.0 0.8 copy-start.1
  0.8 0.7 copy-start
